TPU v7x, 32 devices: a whole 2x2x4 slice. The times are simulated.
32 devices in a mesh: kv: 16 (over z, y, x), tp: 2 (over core).
Axes of the slice: x: 2, y: 2, z: 4, core: 2. Of those that a mesh axis runs over, the one named last changes fastest.
Arguments:
- tokens: bfloat16 [64, 2048], P('tp', 'kv'), may hold values from -24 to 24
- lengths: int32 [16], P('kv'), may hold values from 1 to 4, 40 in all
- memory_state: float32 [16, 16, 128, 128], P('kv', 'tp'), may hold values from -3 to 3
- gain_first: float32 [2048], P('kv'), may hold values from 0.1 to 1.9
- first_gate: bfloat16 [2048, 5120], P('kv', 'tp'), may hold values from -0.125 to 0.125
- first_up: bfloat16 [2048, 5120], P('kv', 'tp'), may hold values from -0.125 to 0.125
- first_down: bfloat16 [5120, 2048], P('tp', 'kv'), may hold values from -0.15625 to 0.15625
- gain_mixer: float32 [2048], P('kv'), may hold values from 0.1 to 1.9
- query_weight: bfloat16 [2048, 2048], P('kv', 'tp'), may hold values from -0.125 to 0.125
- key_weight: bfloat16 [2048, 2048], P('kv', 'tp'), may hold values from -0.125 to 0.125
- value_weight: bfloat16 [2048, 2048], P('kv', 'tp'), may hold values from -0.125 to 0.125
- outgate_weight: bfloat16 [2048, 2048], P('kv', 'tp'), may hold values from -0.125 to 0.125
- beta_weight: bfloat16 [2048, 16], P('kv'), may hold values from -0.125 to 0.125
- decay_weight: bfloat16 [2048, 16], P('kv'), may hold values from -0.125 to 0.125
- decay_rate: float32 [16], P('tp'), may hold values from 0.05 to 4
- decay_bias: float32 [16], P('tp'), may hold values from -3 to 1
- head_gain: float32 [128], replicated, may hold values from 0.1 to 1.9
- out_weight: bfloat16 [2048, 2048], P('tp', 'kv'), may hold values from -0.25 to 0.25
- gain_second: float32 [2048], P('kv'), may hold values from 0.1 to 1.9
- second_gate: bfloat16 [2048, 5120], P('kv', 'tp'), may hold values from -0.125 to 0.125
- second_up: bfloat16 [2048, 5120], P('kv', 'tp'), may hold values from -0.125 to 0.125
- second_down: bfloat16 [5120, 2048], P('tp', 'kv'), may hold values from -0.15625 to 0.15625
Outputs:
- layer_out: bfloat16 [64, 2048], P('tp', 'kv')
- state_out: float32 [16, 16, 128, 128], P('kv', 'tp')
Inputs may be any that keep to these rules, and one draw needn't show every extreme that they name: `lengths`: each sequence's count of live new token slots.
All inputs are finite; a program needn't handle non-finite values. No bound on the sum of `lengths` on one device may be relied on, other than what follows from the above.
Results may differ from a plain program's by a relative error of at most 0.02.
Values may be sent and summed in bfloat16 or wider, within the bound.
A program may use at most 64 MiB of HBM per device.

v0:
```python
import functools

import jax
import jax.numpy as jnp
from jax import lax
from jax.experimental import pallas as pl
from jax.experimental.pallas import tpu as pltpu
from jax.sharding import PartitionSpec as P

MESH = pl.DeviceIdType.MESH
HEAD_DIM = 128
LANES = 128
NEW = 4
EPS = 1e-06
F32 = jnp.float32
BF16 = jnp.bfloat16


def silu(x):
    return x / (1.0 + jnp.exp(-x))


def pieces(total, most):
    return next(k for k in range(most, 0, -1) if total % k == 0)


def swaps(count):
    return count > 2


def chunks_of(total, step):
    return [(c, min(step, total - c)) for c in range(0, total, step)]


def layer_kernel(
    n,
    tps,
    tokens,
    lengths,
    state_hbm,
    gain_first,
    first_gate_hbm,
    first_up_hbm,
    first_down_hbm,
    gain_mixer,
    query_hbm,
    key_hbm,
    value_hbm,
    outgate_hbm,
    beta_weight,
    decay_weight,
    decay_rate,
    decay_bias,
    head_gain,
    out_hbm,
    gain_second,
    second_gate_hbm,
    second_up_hbm,
    second_down_hbm,
    layer_out,
    state_out_hbm,
    first_gate,
    first_up,
    first_down,
    query_w,
    key_w,
    value_w,
    outgate_w,
    out_w,
    second_gate,
    second_up,
    second_down,
    state,
    new_state,
    resid,
    spread_top,
    spread_low,
    arrived,
    natural,
    first_sums,
    mixer_sums,
    second_sums,
    hidden_first,
    hidden_mixer,
    hidden_second,
    pair_first,
    pair_mixer,
    pair_second,
    load_sem,
    send_sem,
    recv_sem,
    pair_sem,
):
    me = lax.axis_index("kv")
    my_tp = lax.axis_index("tp")
    rows, width = resid.shape
    own_rows = rows // tps
    group = hidden_first.shape[0]
    depth = n // group
    my_plane, my_depth = lax.rem(me, group), me // group
    heads = state.shape[0]
    model = n * width

    barrier = pltpu.get_barrier_semaphore()

    def greet_plane(step, carry):
        to = my_depth * group + lax.rem(my_plane + step, group)
        pl.semaphore_signal(barrier, inc=1, device_id={"kv": to}, device_id_type=MESH)
        return carry

    def greet_depth(step, carry):
        to = lax.rem(my_depth + step, depth) * group + my_plane
        pl.semaphore_signal(barrier, inc=1, device_id={"kv": to}, device_id_type=MESH)
        return carry

    def greet_tp(step, carry):
        pl.semaphore_signal(
            barrier, inc=1, device_id={"tp": lax.rem(my_tp + step, tps)}, device_id_type=MESH
        )
        return carry

    lax.fori_loop(1, depth, greet_depth, 0)
    lax.fori_loop(1, group, greet_plane, 0)
    lax.fori_loop(1, tps, greet_tp, 0)

    loads = []
    for at, (src, dst) in enumerate(
        (
            (first_gate_hbm, first_gate),
            (first_up_hbm, first_up),
            (first_down_hbm, first_down),
            (query_hbm, query_w),
            (key_hbm, key_w),
            (value_hbm, value_w),
            (outgate_hbm, outgate_w),
            (state_hbm.at[0], state),
            (out_hbm, out_w),
            (second_gate_hbm, second_gate),
            (second_up_hbm, second_up),
            (second_down_hbm, second_down),
        )
    ):
        load = pltpu.make_async_copy(src, dst, load_sem.at[at])
        load.start()
        loads.append(load)

    spread_rows, half = 2 * rows, NEW
    at_row = lax.broadcasted_iota(jnp.int32, (spread_rows, rows), 0)
    at_col = lax.broadcasted_iota(jnp.int32, (spread_rows, rows), 1)
    source = (at_row // (2 * half)) * half + at_row % half
    top = (at_row % (2 * half)) < half
    hit = source == at_col
    spread_top[...] = jnp.where(hit & top, 1.0, 0.0).astype(BF16)
    spread_low[...] = jnp.where(hit & jnp.logical_not(top), 1.0, 0.0).astype(BF16)

    own = pl.ds(pl.multiple_of(my_tp * own_rows, own_rows), own_rows)
    arrived[own, :] = tokens[...].astype(F32)
    place_row = lax.broadcasted_iota(jnp.int32, (rows, rows), 0)
    place_col = lax.broadcasted_iota(jnp.int32, (rows, rows), 1)
    block = place_row // half
    wanted = ((block % depth) * group + block // depth) * half + place_row % half
    natural[...] = jnp.where(wanted == place_col, 1.0, 0.0).astype(BF16)
    pl.semaphore_wait(barrier, depth - 1 + group - 1 + tps - 1)

    def all_tp(src, dst, stage, part):
        def one(step, carry):
            pltpu.make_async_remote_copy(
                src_ref=src,
                dst_ref=dst,
                send_sem=pair_sem.at[0, stage],
                recv_sem=pair_sem.at[1, stage],
                device_id={"tp": lax.rem(my_tp + step, tps)},
                device_id_type=MESH,
            ).start()
            return carry

        lax.fori_loop(1, tps, one, 0)

        def settle(sem):
            def one_wait(step, carry):
                pltpu.make_async_copy(part, part, sem).wait()
                return carry

            lax.fori_loop(1, tps, one_wait, 0)

        settle(pair_sem.at[1, stage])
        settle(pair_sem.at[0, stage])

    all_tp(arrived.at[own, :], arrived.at[own, :], 0, arrived.at[pl.ds(0, own_rows), :])
    resid[...] = jnp.dot(
        natural[...], arrived[...].astype(BF16), preferred_element_type=F32
    )

    def spread(matrix_top, matrix_low):
        low = jnp.dot(spread_low[...], matrix_low, preferred_element_type=F32)
        high = jnp.dot(spread_top[...], matrix_top, preferred_element_type=F32)
        return high, low

    def norm_operand(gain):
        whole = resid[...]
        squares = jnp.sum(whole * whole, axis=1, keepdims=True)
        operand = (whole * gain[...]).astype(BF16)
        squares_top = squares.astype(BF16)
        squares_low = (squares - squares_top.astype(F32)).astype(BF16)
        high, low = spread(operand, operand)
        sq_high, sq_low = spread(
            jnp.broadcast_to(squares_top.astype(F32), (rows, LANES)).astype(BF16),
            jnp.broadcast_to(squares_low.astype(F32), (rows, LANES)).astype(BF16),
        )
        return high.astype(BF16), low.astype(BF16), sq_high + sq_low

    def rs_first(bufs, sems, c, start, size, swapped):
        send, mid, _, _, swap_mid, _, _, _ = bufs
        cols = pl.ds(start, size)
        if swapped:
            count, place, sem = depth, my_depth, sems + 4
        else:
            count, place, sem = group, my_plane, sems

        def source(to):
            return send.at[:, to, :, cols] if swapped else send.at[to, :, :, cols]

        target = swap_mid.at[place] if swapped else mid.at[place, :, :, cols]
        pltpu.make_async_copy(source(place), target, recv_sem.at[sems, c]).start()

        def one(step, carry):
            to = lax.rem(place + step, count)
            kv = to * group + my_plane if swapped else my_depth * group + to
            pltpu.make_async_remote_copy(
                src_ref=source(to),
                dst_ref=target,
                send_sem=send_sem.at[sem],
                recv_sem=recv_sem.at[sems, c],
                device_id={"kv": kv},
                device_id_type=MESH,
            ).start()
            return carry

        lax.fori_loop(1, count, one, 0)

    def rs_second(bufs, sems, c, start, size, swapped):
        _, mid, red, fin, swap_mid, swap_red, swap_fin, _ = bufs
        if swapped:
            came, kept, last, base = swap_mid, swap_red, swap_fin, 0
            count, place, sem = group, my_plane, sems + 5
        else:
            came, kept, last, base = mid, red, fin, start
            count, place, sem = depth, my_depth, sems + 1
        cols = pl.ds(base, size)
        part = came.at[:, :, :, cols]
        pltpu.make_async_copy(part, part, recv_sem.at[sems, c]).wait()
        for d in range(count):
            for at, wide in chunks_of(size, 512):
                span_at = slice(base + at, base + at + wide)
                value = came[0, d, :, span_at].astype(F32)
                for g in range(1, came.shape[0]):
                    value = value + came[g, d, :, span_at].astype(F32)
                kept[d, :, span_at] = value.astype(BF16)
        pltpu.make_async_copy(
            kept.at[place, :, cols], last.at[place, :, cols], recv_sem.at[sems + 1, c]
        ).start()

        def one(step, carry):
            to = lax.rem(place + step, count)
            kv = my_depth * group + to if swapped else to * group + my_plane
            pltpu.make_async_remote_copy(
                src_ref=kept.at[to, :, cols],
                dst_ref=last.at[place, :, cols],
                send_sem=send_sem.at[sem],
                recv_sem=recv_sem.at[sems + 1, c],
                device_id={"kv": kv},
                device_id_type=MESH,
            ).start()
            return carry

        lax.fori_loop(1, count, one, 0)

    def rs_wait(bufs, sems, c, start, size, swapped):
        part = bufs[6] if swapped else bufs[3].at[:, :, pl.ds(start, size)]
        pltpu.make_async_copy(part, part, recv_sem.at[sems + 1, c]).wait()

    def ag_depth(bufs, sems, c, start, size):
        buffer = bufs[7]
        mine = buffer.at[my_plane, my_depth, :, pl.ds(start, size)]

        def one(step, carry):
            pltpu.make_async_remote_copy(
                src_ref=mine,
                dst_ref=mine,
                send_sem=send_sem.at[sems + 2],
                recv_sem=recv_sem.at[sems + 2, c],
                device_id={"kv": lax.rem(my_depth + step, depth) * group + my_plane},
                device_id_type=MESH,
            ).start()
            return carry

        lax.fori_loop(1, depth, one, 0)

    def ag_plane(bufs, sems, c, start, size):
        buffer = bufs[7]
        cols = pl.ds(start, size)
        part = buffer.at[0, pl.ds(0, depth - 1), :, cols]
        pltpu.make_async_copy(part, part, recv_sem.at[sems + 2, c]).wait()
        mine = buffer.at[my_plane, :, :, cols]

        def one(step, carry):
            pltpu.make_async_remote_copy(
                src_ref=mine,
                dst_ref=mine,
                send_sem=send_sem.at[sems + 3],
                recv_sem=recv_sem.at[sems + 3, c],
                device_id={"kv": my_depth * group + lax.rem(my_plane + step, group)},
                device_id_type=MESH,
            ).start()
            return carry

        lax.fori_loop(1, group, one, 0)

    def ag_wait(bufs, sems, c, start, size):
        part = bufs[7].at[pl.ds(0, group - 1), :, :, pl.ds(start, size)]
        pltpu.make_async_copy(part, part, recv_sem.at[sems + 3, c]).wait()

    def all_sent(bufs, sems):
        send, mid, red, fin, swap_mid, swap_red, swap_fin, buffer = bufs
        parts = [
            mid.at[pl.ds(0, group - 1)],
            fin.at[pl.ds(0, depth - 1)],
            buffer.at[0, pl.ds(0, depth - 1)],
            buffer.at[pl.ds(0, group - 1)],
        ]
        if mid.shape[3] < send.shape[3]:
            parts += [swap_mid.at[pl.ds(0, depth - 1)], swap_fin.at[pl.ds(0, group - 1)]]
        for at, part in enumerate(parts):
            pltpu.make_async_copy(part, part, send_sem.at[sems + at]).wait()

    def put(send, start, size, value):
        send[:, :, :, start : start + size] = value.reshape(group, depth, 2 * half, size).astype(
            BF16
        )

    def total(bufs, start, size):
        fin, begin = bufs[3], start
        if start >= fin.shape[2]:
            fin, begin = bufs[6], start - fin.shape[2]
        value = fin[0, :, begin : begin + size].astype(F32)
        for k in range(1, fin.shape[0]):
            value = value + fin[k, :, begin : begin + size].astype(F32)
        return value

    def inverse_rms(bufs):
        squares = total(bufs, 0, LANES)
        return lax.rsqrt((squares[:half] + squares[half:]) / model + EPS)

    def stacked(buffer, start, size):
        flat = buffer[:, :, :, start : start + size].astype(F32).reshape(rows, size)
        return flat.astype(BF16)

    def in_order(count):
        order = list(range(count))
        if swaps(count):
            order = order[: count - 2] + [count - 1, count - 2]
        return [(stage, c) for stage in range(4) for c in order]

    def in_issue(count):
        order = list(range(count))
        return order[-1:] + order[:-1] if swaps(count) else order

    def feed_forward(gain, gate, up, down, waits, bufs, pair, sems, tp_sems):
        send, hidden = bufs[0], bufs[7]
        high, low, squares = norm_operand(gain)
        units = gate.shape[1]
        count = pieces(units // LANES, 4)
        size = units // count
        put(send, 0, LANES, squares)
        waits[0].wait()
        waits[1].wait()

        def sums_at(c):
            swapped = swaps(count) and c == count - 1
            return (0, LANES + size, False) if c == 0 else (LANES + c * size, size, swapped)

        for c in in_issue(count):
            for at, wide in chunks_of(size, 512):
                lo = c * size + at
                put(
                    send,
                    LANES + lo,
                    wide,
                    jnp.dot(high, gate[:, lo : lo + wide], preferred_element_type=F32)
                    + jnp.dot(low, up[:, lo : lo + wide], preferred_element_type=F32),
                )
            rs_first(bufs, sems, c, *sums_at(c))
        branch = jnp.zeros((rows, width), F32)
        scale, down_ready = None, []
        for stage, c in in_order(count):
            if stage == 0:
                rs_second(bufs, sems, c, *sums_at(c))
            elif stage == 1:
                rs_wait(bufs, sems, c, *sums_at(c))
                if c == 0:
                    scale = inverse_rms(bufs)
                for at, wide in chunks_of(size, LANES):
                    lo = c * size + at
                    both = total(bufs, LANES + lo, wide)
                    hidden[my_plane, my_depth, :, lo : lo + wide] = (
                        silu(both[:half] * scale) * (both[half:] * scale)
                    ).astype(BF16)
                ag_depth(bufs, sems, c, c * size, size)
            elif stage == 2:
                ag_plane(bufs, sems, c, c * size, size)
            else:
                ag_wait(bufs, sems, c, c * size, size)
                if not down_ready:
                    down_ready.append(waits[2].wait())
                branch = branch + jnp.dot(
                    stacked(hidden, c * size, size),
                    down[c * size : (c + 1) * size, :],
                    preferred_element_type=F32,
                )
        pair[my_tp] = branch
        all_tp(pair.at[my_tp], pair.at[my_tp], tp_sems, pair.at[0])
        branch = pair[0]
        for t in range(1, tps):
            branch = branch + pair[t]
        resid[...] = (resid[...] + 0.5 * branch).astype(BF16).astype(F32)

    first_bufs = (*first_sums, hidden_first)
    mixer_bufs = (*mixer_sums, hidden_mixer)
    second_bufs = (*second_sums, hidden_second)
    send_mixer = mixer_sums[0]
    feed_forward(
        gain_first, first_gate, first_up, first_down, loads[0:3],
        first_bufs, pair_first, 0, 1,
    )

    high, low, squares = norm_operand(gain_mixer)
    all_heads = beta_weight.shape[0]
    across = (((1,), (1,)), ((), ()))
    put(send_mixer, 0, LANES, squares)
    send_mixer[:, :, :, LANES : 2 * LANES] = jnp.zeros((group, depth, 2 * half, LANES), BF16)
    small = lax.dot_general(
        high, beta_weight[...], across, preferred_element_type=F32
    ) + lax.dot_general(low, decay_weight[...], across, preferred_element_type=F32)
    put(send_mixer, LANES, all_heads, small)
    for load in loads[3:7]:
        load.wait()
    count = pieces(heads, 4)
    batch = heads // count
    size = batch * HEAD_DIM

    def mixed_at(c):
        start = 2 * LANES + 2 * c * size
        swapped = swaps(count) and c == count - 1
        return (0, 2 * LANES + 2 * size, False) if c == 0 else (start, 2 * size, swapped)

    for c in in_issue(count):
        for at, (first, second) in enumerate(((query_w, value_w), (key_w, outgate_w))):
            lo = c * size
            put(
                send_mixer,
                2 * LANES + (2 * c + at) * size,
                size,
                jnp.dot(high, first[:, lo : lo + size], preferred_element_type=F32)
                + jnp.dot(low, second[:, lo : lo + size], preferred_element_type=F32),
            )
        rs_first(mixer_bufs, 6, c, *mixed_at(c))
    lane = lax.broadcasted_iota(jnp.int32, (half, LANES), 1)
    slot = lax.broadcasted_iota(jnp.int32, (half, LANES), 0)
    live = jnp.where(slot < lengths[0], 1.0, 0.0)
    scale, logits = None, None
    branch = jnp.zeros((rows, width), F32)
    for stage, c in in_order(count):
        if stage == 0:
            rs_second(mixer_bufs, 6, c, *mixed_at(c))
            continue
        if stage == 2:
            ag_plane(mixer_bufs, 6, c, c * size, size)
            continue
        if stage == 3:
            ag_wait(mixer_bufs, 6, c, c * size, size)
            if c == 0:
                loads[8].wait()
            branch = branch + jnp.dot(
                stacked(hidden_mixer, c * size, size),
                out_w[c * size : (c + 1) * size, :],
                preferred_element_type=F32,
            )
            continue
        rs_wait(mixer_bufs, 6, c, *mixed_at(c))
        if c == 0:
            scale = inverse_rms(mixer_bufs)
            logits = total(mixer_bufs, LANES, LANES)
            loads[7].wait()
        for h in range(c * batch, (c + 1) * batch):
            base = 2 * LANES + 2 * c * size + (h - c * batch) * HEAD_DIM
            both = total(mixer_bufs, base, HEAD_DIM)
            query, value = silu(both[:half] * scale), silu(both[half:] * scale)
            both = total(mixer_bufs, base + size, HEAD_DIM)
            keyvec, outgate = silu(both[:half] * scale), silu(both[half:] * scale)
            query = query * lax.rsqrt(jnp.sum(query * query, axis=1, keepdims=True) + EPS)
            query = query * HEAD_DIM ** (-0.5)
            keyvec = keyvec * lax.rsqrt(jnp.sum(keyvec * keyvec, axis=1, keepdims=True) + EPS)
            mine = lane == my_tp * heads + h
            beta_logit = jnp.sum(jnp.where(mine, logits[:half] * scale, 0.0), axis=1, keepdims=True)
            decay_logit = jnp.sum(jnp.where(mine, logits[half:] * scale, 0.0), axis=1, keepdims=True)
            beta_logit = jnp.broadcast_to(beta_logit, (half, LANES))
            decay_logit = jnp.broadcast_to(decay_logit, (half, LANES)) + decay_bias[0, h]
            beta = live / (1.0 + jnp.exp(-beta_logit))
            soft = jnp.maximum(decay_logit, 0.0) + jnp.log(1.0 + jnp.exp(-jnp.abs(decay_logit)))
            decay = -decay_rate[0, h] * soft * live
            reach = jnp.zeros_like(decay)
            for i in range(NEW):
                reach = reach + jnp.where(slot >= i, decay[i : i + 1], 0.0)
            before = jnp.exp(reach)
            old = state[h]
            held = jnp.dot(
                jnp.concatenate([keyvec, query], axis=0),
                old,
                precision=lax.Precision.HIGHEST,
                preferred_element_type=F32,
            )
            update = beta * (value - before * held[:half])
            output = before * held[half:]
            for i in range(NEW):
                between = jnp.where(slot >= i, jnp.exp(jnp.minimum(reach - reach[i : i + 1], 0.0)), 0.0)
                row = keyvec[i : i + 1]
                alike = jnp.sum(keyvec * row, axis=1, keepdims=True)
                fixed = update[i : i + 1]
                update = update - jnp.where(slot > i, beta * between * alike * fixed, 0.0)
                output = output + between * jnp.sum(query * row, axis=1, keepdims=True) * fixed
            last = reach[NEW - 1 : NEW]
            gained = update * jnp.exp(last - reach)
            zero = jnp.zeros_like(keyvec)
            new_state[h] = old * jnp.exp(last) + lax.dot_general(
                jnp.concatenate([keyvec, zero], axis=0),
                jnp.concatenate([gained, zero], axis=0),
                (((0,), (0,)), ((), ())),
                precision=lax.Precision.HIGHEST,
                preferred_element_type=F32,
            )
            output = output * live
            output = output * lax.rsqrt(jnp.mean(output * output, axis=1, keepdims=True) + EPS)
            output = output * head_gain[...] * outgate
            hidden_mixer[my_plane, my_depth, :, h * HEAD_DIM : (h + 1) * HEAD_DIM] = output.astype(
                BF16
            )
        ag_depth(mixer_bufs, 6, c, c * size, size)
    save = pltpu.make_async_copy(new_state, state_out_hbm.at[0], load_sem.at[12])
    save.start()
    pair_mixer[my_tp] = branch
    all_tp(pair_mixer.at[my_tp], pair_mixer.at[my_tp], 2, pair_mixer.at[0])
    branch = pair_mixer[0]
    for t in range(1, tps):
        branch = branch + pair_mixer[t]
    resid[...] = (resid[...] + branch).astype(BF16).astype(F32)

    feed_forward(
        gain_second, second_gate, second_up, second_down, loads[9:12],
        second_bufs, pair_second, 12, 3,
    )
    arrived[...] = lax.dot_general(
        natural[...], resid[...].astype(BF16), (((0,), (0,)), ((), ())), preferred_element_type=F32
    )
    layer_out[...] = arrived[own, :].astype(BF16)
    save.wait()
    all_sent(first_bufs, 0)
    all_sent(mixer_bufs, 6)
    all_sent(second_bufs, 12)


def solution(mesh):
    n, tps = mesh.shape["kv"], mesh.shape["tp"]

    def on_device(
        tokens,
        lengths,
        memory_state,
        gain_first,
        first_gate,
        first_up,
        first_down,
        gain_mixer,
        query_weight,
        key_weight,
        value_weight,
        outgate_weight,
        beta_weight,
        decay_weight,
        decay_rate,
        decay_bias,
        head_gain,
        out_weight,
        gain_second,
        second_gate,
        second_up,
        second_down,
    ):
        rows = tokens.shape[0] * tps
        width = tokens.shape[1]
        units = first_gate.shape[1]
        span = query_weight.shape[1]
        group = pieces(n, 4)
        depth = n // group
        half_parts = pieces(units // LANES, 4)
        mixer_parts = pieces(memory_state.shape[1], 4)
        vmem = pl.BlockSpec(memory_space=pltpu.VMEM)
        smem = pl.BlockSpec(memory_space=pltpu.SMEM)
        hbm = pl.BlockSpec(memory_space=pl.ANY)

        def like(array):
            return pltpu.VMEM(array.shape, array.dtype)

        def owners(before, parts, each):
            last = each if swaps(parts) else LANES
            columns = before + parts * each
            kept = columns - (last if swaps(parts) else 0)
            return (
                pltpu.VMEM((group, depth, 2 * NEW, columns), BF16),
                pltpu.VMEM((group, depth, 2 * NEW, kept), BF16),
                pltpu.VMEM((depth, 2 * NEW, kept), BF16),
                pltpu.VMEM((depth, 2 * NEW, kept), BF16),
                pltpu.VMEM((depth, group, 2 * NEW, last), BF16),
                pltpu.VMEM((group, 2 * NEW, last), BF16),
                pltpu.VMEM((group, 2 * NEW, last), BF16),
            )

        def gathered(columns):
            return pltpu.VMEM((group, depth, NEW, columns), BF16)

        def pairs():
            return pltpu.VMEM((tps, rows, width), F32)

        return pl.pallas_call(
            functools.partial(layer_kernel, n, tps),
            name="layer",
            out_shape=(
                jax.ShapeDtypeStruct(tokens.shape, BF16),
                jax.ShapeDtypeStruct(memory_state.shape, F32),
            ),
            in_specs=[
                vmem, smem, hbm, vmem, hbm, hbm, hbm, vmem, hbm, hbm, hbm, hbm,
                vmem, vmem, smem, smem, vmem, hbm, vmem, hbm, hbm, hbm,
            ],
            out_specs=(vmem, hbm),
            scratch_shapes=[
                like(first_gate),
                like(first_up),
                like(first_down),
                like(query_weight),
                like(key_weight),
                like(value_weight),
                like(outgate_weight),
                like(out_weight),
                like(second_gate),
                like(second_up),
                like(second_down),
                pltpu.VMEM(memory_state.shape[1:], F32),
                pltpu.VMEM(memory_state.shape[1:], F32),
                pltpu.VMEM((rows, width), F32),
                pltpu.VMEM((2 * rows, rows), BF16),
                pltpu.VMEM((2 * rows, rows), BF16),
                pltpu.VMEM((rows, width), F32),
                pltpu.VMEM((rows, rows), BF16),
                owners(LANES, half_parts, units // half_parts),
                owners(2 * LANES, mixer_parts, 2 * span // mixer_parts),
                owners(LANES, half_parts, units // half_parts),
                gathered(units),
                gathered(span),
                gathered(units),
                pairs(),
                pairs(),
                pairs(),
                pltpu.SemaphoreType.DMA((13,)),
                pltpu.SemaphoreType.DMA((18,)),
                pltpu.SemaphoreType.DMA((18, 4)),
                pltpu.SemaphoreType.DMA((2, 4)),
            ],
            compiler_params=pltpu.CompilerParams(
                collective_id=0,
                has_side_effects=True,
                vmem_limit_bytes=60 * 1024 * 1024,
            ),
        )(
            tokens,
            lengths,
            memory_state,
            gain_first.reshape(1, -1),
            first_gate,
            first_up,
            first_down,
            gain_mixer.reshape(1, -1),
            query_weight,
            key_weight,
            value_weight,
            outgate_weight,
            beta_weight.T,
            decay_weight.T,
            decay_rate.reshape(1, -1),
            decay_bias.reshape(1, -1),
            head_gain.reshape(1, -1),
            out_weight,
            gain_second.reshape(1, -1),
            second_gate,
            second_up,
            second_down,
        )

    in_specs = (
        P("tp", "kv"),
        P("kv"),
        P("kv", "tp", None, None),
        P("kv"),
        P("kv", "tp"),
        P("kv", "tp"),
        P("tp", "kv"),
        P("kv"),
        P("kv", "tp"),
        P("kv", "tp"),
        P("kv", "tp"),
        P("kv", "tp"),
        P("kv", None),
        P("kv", None),
        P("tp"),
        P("tp"),
        P(),
        P("tp", "kv"),
        P("kv"),
        P("kv", "tp"),
        P("kv", "tp"),
        P("tp", "kv"),
    )
    out_specs = (P("tp", "kv"), P("kv", "tp", None, None))
    return jax.shard_map(
        on_device, mesh=mesh, in_specs=in_specs, out_specs=out_specs, check_vma=False
    )
```

profile of v0, /device:TPU:0, one launch (start us, length us, event | category | flops | bytes accessed | tf_op | source)
XLA Modules:
  0.0 76.4 jit_solution(11979332085136586585)
XLA Ops:
  1.3 72.0 %layer.1 = (bf16[32,128]{1,0:T(8,128)(2,1)}, f32[1,8,128,128]{3,2,1,0:T(8,128)}) custom-call(bf16[32,128]{1,0:T(8,128)(2,1)} %tokens.1, s32[1]{0:T(128)S(6)} %copy.26.lengths, f32[1,8,128,128]{3,2,1,0:T(8,128)} %state_hbm.1, f32[1,128]{1,0:T(1,128)} %bitcast.10, bf16[128,2560]{1,0:T(8,128)(2,1)} %first_gate_hbm.1, bf16[128,2560]{1,0:T(8,128)(2,1)} %first_up_hbm.1, ...), custom_call_target="tpu_custom_call" | custom-call | tf_op jit(solution)/shard_map/layer/pallas_call | solution.py:633
  73.3 1.3 %copy.27 = bf16[32,128]{1,0:T(8,128)(2,1)} copy(bf16[32,128]{1,0:T(8,128)(2,1)} %get-tuple-element.4) | data formatting | bytes 16384
  74.6 1.9 %copy.28 = f32[1,8,128,128]{3,2,1,0:T(8,128)} copy(f32[1,8,128,128]{3,2,1,0:T(8,128)} %get-tuple-element.5) | data formatting | bytes 1048576
where the time goes:
time: 76.7 us; the launch traced here: 76.4 us
  Pallas kernels  72 us (94%)
  local copies, waits for them, and re-layouts  3.17 us (4%)
  between operations  1.29 us (2%)
    pallas_call x1, Pallas kernels, on_device(): pl.pallas_call(functools.partial(layer_kernel, n, tps), name='layer', out...  72 us
    unnamed x2, local copies, waits for them, and re-layouts  3.17 us

commit v1 on v0

--- a/solution.py
+++ b/solution.py
@@ -26,6 +26,10 @@
 
 def swaps(count):
     return count > 2
+
+
+def early_of(count):
+    return min(1, count - 1 - int(swaps(count)))
 
 
 def chunks_of(total, step):
@@ -90,6 +94,8 @@
     send_sem,
     recv_sem,
     pair_sem,
+    early_sem,
+    turn_sem,
 ):
     me = lax.axis_index("kv")
     my_tp = lax.axis_index("tp")
@@ -100,6 +106,9 @@
     my_plane, my_depth = lax.rem(me, group), me // group
     heads = state.shape[0]
     model = n * width
+    paired = tps % 2 == 0
+    late = lax.rem(my_tp, 2) == 1
+    partner = my_tp + 1 - 2 * lax.rem(my_tp, 2)
 
     barrier = pltpu.get_barrier_semaphore()
 
@@ -210,8 +219,15 @@
         return high.astype(BF16), low.astype(BF16), sq_high + sq_low
 
     def rs_first(bufs, sems, c, start, size, swapped):
-        send, mid, _, _, swap_mid, _, _, _ = bufs
+        send, mid, _, _, swap_mid, _, _, _, _, _ = bufs
         cols = pl.ds(start, size)
+        stage = sems // 6
+        if paired and not swapped and c == 0:
+
+            @pl.when(late)
+            def _():
+                pl.semaphore_wait(turn_sem.at[stage], 1)
+
         if swapped:
             count, place, sem = depth, my_depth, sems + 4
         else:
@@ -220,6 +236,7 @@
         def source(to):
             return send.at[:, to, :, cols] if swapped else send.at[to, :, :, cols]
 
+        early = not swapped and c == early_of(bufs[8])
         target = swap_mid.at[place] if swapped else mid.at[place, :, :, cols]
         pltpu.make_async_copy(source(place), target, recv_sem.at[sems, c]).start()
 
@@ -229,7 +246,7 @@
             pltpu.make_async_remote_copy(
                 src_ref=source(to),
                 dst_ref=target,
-                send_sem=send_sem.at[sem],
+                send_sem=early_sem.at[stage] if early else send_sem.at[sem],
                 recv_sem=recv_sem.at[sems, c],
                 device_id={"kv": kv},
                 device_id_type=MESH,
@@ -238,8 +255,22 @@
 
         lax.fori_loop(1, count, one, 0)
 
+    def early_part(bufs, start, size):
+        return bufs[1].at[pl.ds(0, group - 1), :, :, pl.ds(start, size)]
+
+    def hand_over(bufs, sems, start, size):
+        part = early_part(bufs, start, size)
+        pltpu.make_async_copy(part, part, early_sem.at[sems // 6]).wait()
+        if paired:
+
+            @pl.when(jnp.logical_not(late))
+            def _():
+                pl.semaphore_signal(
+                    turn_sem.at[sems // 6], inc=1, device_id={"tp": partner}, device_id_type=MESH
+                )
+
     def rs_second(bufs, sems, c, start, size, swapped):
-        _, mid, red, fin, swap_mid, swap_red, swap_fin, _ = bufs
+        _, mid, red, fin, swap_mid, swap_red, swap_fin, _, _, _ = bufs
         if swapped:
             came, kept, last, base = swap_mid, swap_red, swap_fin, 0
             count, place, sem = group, my_plane, sems + 5
@@ -321,9 +352,9 @@
         pltpu.make_async_copy(part, part, recv_sem.at[sems + 3, c]).wait()
 
     def all_sent(bufs, sems):
-        send, mid, red, fin, swap_mid, swap_red, swap_fin, buffer = bufs
+        send, mid, red, fin, swap_mid, swap_red, swap_fin, buffer, _, width = bufs
         parts = [
-            mid.at[pl.ds(0, group - 1)],
+            mid.at[pl.ds(0, group - 1), :, :, pl.ds(0, mid.shape[3] - width)],
             fin.at[pl.ds(0, depth - 1)],
             buffer.at[0, pl.ds(0, depth - 1)],
             buffer.at[pl.ds(0, group - 1)],
@@ -331,7 +362,8 @@
         if mid.shape[3] < send.shape[3]:
             parts += [swap_mid.at[pl.ds(0, depth - 1)], swap_fin.at[pl.ds(0, group - 1)]]
         for at, part in enumerate(parts):
-            pltpu.make_async_copy(part, part, send_sem.at[sems + at]).wait()
+            if min(part.shape) > 0:
+                pltpu.make_async_copy(part, part, send_sem.at[sems + at]).wait()
 
     def put(send, start, size, value):
         send[:, :, :, start : start + size] = value.reshape(group, depth, 2 * half, size).astype(
@@ -390,6 +422,7 @@
                     + jnp.dot(low, up[:, lo : lo + wide], preferred_element_type=F32),
                 )
             rs_first(bufs, sems, c, *sums_at(c))
+        hand_over(bufs, sems, *sums_at(early_of(count))[:2])
         branch = jnp.zeros((rows, width), F32)
         scale, down_ready = None, []
         for stage, c in in_order(count):
@@ -424,9 +457,19 @@
             branch = branch + pair[t]
         resid[...] = (resid[...] + 0.5 * branch).astype(BF16).astype(F32)
 
-    first_bufs = (*first_sums, hidden_first)
-    mixer_bufs = (*mixer_sums, hidden_mixer)
-    second_bufs = (*second_sums, hidden_second)
+    half_count = pieces(first_gate.shape[1] // LANES, 4)
+    half_size = first_gate.shape[1] // half_count
+    mixer_count = pieces(heads, 4)
+    mixer_size = 2 * heads * HEAD_DIM // mixer_count
+
+    def early_width(before, parts, each):
+        return each if early_of(parts) else before + each
+
+    half_early = (half_count, early_width(LANES, half_count, half_size))
+    mixer_early = (mixer_count, early_width(2 * LANES, mixer_count, mixer_size))
+    first_bufs = (*first_sums, hidden_first, *half_early)
+    mixer_bufs = (*mixer_sums, hidden_mixer, *mixer_early)
+    second_bufs = (*second_sums, hidden_second, *half_early)
     send_mixer = mixer_sums[0]
     feed_forward(
         gain_first, first_gate, first_up, first_down, loads[0:3],
@@ -464,6 +507,7 @@
                 + jnp.dot(low, second[:, lo : lo + size], preferred_element_type=F32),
             )
         rs_first(mixer_bufs, 6, c, *mixed_at(c))
+    hand_over(mixer_bufs, 6, *mixed_at(early_of(count))[:2])
     lane = lax.broadcasted_iota(jnp.int32, (half, LANES), 1)
     slot = lax.broadcasted_iota(jnp.int32, (half, LANES), 0)
     live = jnp.where(slot < lengths[0], 1.0, 0.0)
@@ -674,6 +718,8 @@
                 pltpu.SemaphoreType.DMA((18,)),
                 pltpu.SemaphoreType.DMA((18, 4)),
                 pltpu.SemaphoreType.DMA((2, 4)),
+                pltpu.SemaphoreType.DMA((3,)),
+                pltpu.SemaphoreType.REGULAR((3,)),
             ],
             compiler_params=pltpu.CompilerParams(
                 collective_id=0,

time: 76.7 us -> 71.7 us (0.935)
  Pallas kernels: 72 us -> 67 us
    pallas_call x1, Pallas kernels: 72 us -> 67 us  [on_device(): pl.pallas_call(functools.partial(layer_kernel, n, tps), name='layer', out...]
where the time goes in v1:
time: 71.7 us; the launch traced here: 71.5 us
  Pallas kernels  67 us (93%)
  local copies, waits for them, and re-layouts  3.17 us (4%)
  between operations  1.29 us (2%)
    pallas_call x1, Pallas kernels, on_device(): pl.pallas_call(functools.partial(layer_kernel, n, tps), name='layer', out...  67 us
    unnamed x2, local copies, waits for them, and re-layouts  3.17 us

profile of v1, /device:TPU:0, one launch (start us, length us, event | category | flops | bytes accessed | tf_op | source)
XLA Modules:
  0.0 71.5 jit_solution(5971506045022734398)
XLA Ops:
  1.3 67.0 %layer.1 = (bf16[32,128]{1,0:T(8,128)(2,1)}, f32[1,8,128,128]{3,2,1,0:T(8,128)}) custom-call(bf16[32,128]{1,0:T(8,128)(2,1)} %tokens.1, s32[1]{0:T(128)S(6)} %copy.26.lengths, f32[1,8,128,128]{3,2,1,0:T(8,128)} %state_hbm.1, f32[1,128]{1,0:T(1,128)} %bitcast.10, bf16[128,2560]{1,0:T(8,128)(2,1)} %first_gate_hbm.1, bf16[128,2560]{1,0:T(8,128)(2,1)} %first_up_hbm.1, ...), custom_call_target="tpu_custom_call" | custom-call | tf_op jit(solution)/shard_map/layer/pallas_call | solution.py:677
  68.3 1.3 %copy.27 = bf16[32,128]{1,0:T(8,128)(2,1)} copy(bf16[32,128]{1,0:T(8,128)(2,1)} %get-tuple-element.4) | data formatting | bytes 16384
  69.6 1.9 %copy.28 = f32[1,8,128,128]{3,2,1,0:T(8,128)} copy(f32[1,8,128,128]{3,2,1,0:T(8,128)} %get-tuple-element.5) | data formatting | bytes 1048576

commit v2 on v1

--- a/solution.py
+++ b/solution.py
@@ -12,6 +12,9 @@
 LANES = 128
 NEW = 4
 EPS = 1e-06
+EARLY = 1
+HALF_DIRECT = 2
+MIXER_DIRECT = 4
 F32 = jnp.float32
 BF16 = jnp.bfloat16
 
@@ -29,40 +32,61 @@
 
 
 def early_of(count):
-    return min(1, count - 1 - int(swaps(count)))
+    return min(EARLY, count - 1 - int(swaps(count)))
 
 
 def chunks_of(total, step):
     return [(c, min(step, total - c)) for c in range(0, total, step)]
+
+
+def put_out(layer, state, layer_hbm, state_hbm, sem):
+    moves = [
+        pltpu.make_async_copy(src, dst, sem.at[at])
+        for at, (src, dst) in enumerate(((layer, layer_hbm), (state, state_hbm)))
+    ]
+    for move in moves:
+        move.start()
+    for move in moves:
+        move.wait()
 
 
 def layer_kernel(
     n,
     tps,
-    tokens,
-    lengths,
+    tokens_hbm,
+    lengths_hbm,
     state_hbm,
-    gain_first,
+    gain_first_hbm,
     first_gate_hbm,
     first_up_hbm,
     first_down_hbm,
-    gain_mixer,
+    gain_mixer_hbm,
     query_hbm,
     key_hbm,
     value_hbm,
     outgate_hbm,
+    beta_hbm,
+    decay_hbm,
+    rate_hbm,
+    bias_hbm,
+    head_gain_hbm,
+    out_hbm,
+    gain_second_hbm,
+    second_gate_hbm,
+    second_up_hbm,
+    second_down_hbm,
+    layer_out,
+    new_state,
+    tokens,
+    lengths,
+    gain_first,
+    gain_mixer,
     beta_weight,
     decay_weight,
     decay_rate,
     decay_bias,
     head_gain,
-    out_hbm,
     gain_second,
-    second_gate_hbm,
-    second_up_hbm,
-    second_down_hbm,
-    layer_out,
-    state_out_hbm,
     first_gate,
     first_up,
     first_down,
@@ -75,7 +99,6 @@
     second_up,
     second_down,
     state,
-    new_state,
     resid,
     spread_top,
     spread_low,
@@ -96,6 +119,7 @@
     pair_sem,
     early_sem,
     turn_sem,
+    small_sem,
 ):
     me = lax.axis_index("kv")
     my_tp = lax.axis_index("tp")
@@ -131,6 +155,25 @@
     lax.fori_loop(1, depth, greet_depth, 0)
     lax.fori_loop(1, group, greet_plane, 0)
     lax.fori_loop(1, tps, greet_tp, 0)
+
+    smalls = []
+    for at, (src, dst) in enumerate(
+        (
+            (tokens_hbm, tokens),
+            (gain_first_hbm, gain_first),
+            (gain_mixer_hbm, gain_mixer),
+            (beta_hbm, beta_weight),
+            (decay_hbm, decay_weight),
+            (rate_hbm, decay_rate),
+            (bias_hbm, decay_bias),
+            (lengths_hbm, lengths),
+            (head_gain_hbm, head_gain),
+            (gain_second_hbm, gain_second),
+        )
+    ):
+        small = pltpu.make_async_copy(src, dst, small_sem.at[at])
+        small.start()
+        smalls.append(small)
 
     loads = []
     for at, (src, dst) in enumerate(
@@ -162,6 +205,7 @@
     spread_top[...] = jnp.where(hit & top, 1.0, 0.0).astype(BF16)
     spread_low[...] = jnp.where(hit & jnp.logical_not(top), 1.0, 0.0).astype(BF16)
 
+    smalls[0].wait()
     own = pl.ds(pl.multiple_of(my_tp * own_rows, own_rows), own_rows)
     arrived[own, :] = tokens[...].astype(F32)
     place_row = lax.broadcasted_iota(jnp.int32, (rows, rows), 0)
@@ -327,11 +371,29 @@
 
         lax.fori_loop(1, depth, one, 0)
 
+    def ag_direct(bufs, sems, c, start, size):
+        buffer = bufs[7]
+        mine = buffer.at[my_plane, my_depth, :, pl.ds(start, size)]
+
+        def one(step, carry):
+            far, across = step // (group - 1), 1 + lax.rem(step, group - 1)
+            to_depth = lax.rem(my_depth + 1 + far, depth)
+            to_plane = lax.rem(my_plane + across, group)
+            pltpu.make_async_remote_copy(
+                src_ref=mine,
+                dst_ref=mine,
+                send_sem=send_sem.at[sems + 3],
+                recv_sem=recv_sem.at[sems + 3, c],
+                device_id={"kv": to_depth * group + to_plane},
+                device_id_type=MESH,
+            ).start()
+            return carry
+
+        lax.fori_loop(0, depth * (group - 1), one, 0)
+
     def ag_plane(bufs, sems, c, start, size):
         buffer = bufs[7]
         cols = pl.ds(start, size)
-        part = buffer.at[0, pl.ds(0, depth - 1), :, cols]
-        pltpu.make_async_copy(part, part, recv_sem.at[sems + 2, c]).wait()
         mine = buffer.at[my_plane, :, :, cols]
 
         def one(step, carry):
@@ -346,6 +408,10 @@
             return carry
 
         lax.fori_loop(1, group, one, 0)
+
+    def ag_near(bufs, sems, c, start, size):
+        part = bufs[7].at[0, pl.ds(0, depth - 1), :, pl.ds(start, size)]
+        pltpu.make_async_copy(part, part, recv_sem.at[sems + 2, c]).wait()
 
     def ag_wait(bufs, sems, c, start, size):
         part = bufs[7].at[pl.ds(0, group - 1), :, :, pl.ds(start, size)]
@@ -393,12 +459,17 @@
             order = order[: count - 2] + [count - 1, count - 2]
         return [(stage, c) for stage in range(4) for c in order]
 
+    def last_of(count, most):
+        return [c for _, c in in_order(count)][:count][max(0, count - most) :]
+
     def in_issue(count):
         order = list(range(count))
         return order[-1:] + order[:-1] if swaps(count) else order
 
-    def feed_forward(gain, gate, up, down, waits, bufs, pair, sems, tp_sems):
+    def feed_forward(before, gain, gate, up, down, waits, bufs, pair, sems, tp_sems):
         send, hidden = bufs[0], bufs[7]
+        for ready in before:
+            ready.wait()
         high, low, squares = norm_operand(gain)
         units = gate.shape[1]
         count = pieces(units // LANES, 4)
@@ -424,6 +495,7 @@
             rs_first(bufs, sems, c, *sums_at(c))
         hand_over(bufs, sems, *sums_at(early_of(count))[:2])
         branch = jnp.zeros((rows, width), F32)
+        direct = last_of(count, HALF_DIRECT)
         scale, down_ready = None, []
         for stage, c in in_order(count):
             if stage == 0:
@@ -439,9 +511,15 @@
                         silu(both[:half] * scale) * (both[half:] * scale)
                     ).astype(BF16)
                 ag_depth(bufs, sems, c, c * size, size)
+                if c in direct:
+                    ag_direct(bufs, sems, c, c * size, size)
             elif stage == 2:
-                ag_plane(bufs, sems, c, c * size, size)
+                if c not in direct:
+                    ag_near(bufs, sems, c, c * size, size)
+                    ag_plane(bufs, sems, c, c * size, size)
             else:
+                if c in direct:
+                    ag_near(bufs, sems, c, c * size, size)
                 ag_wait(bufs, sems, c, c * size, size)
                 if not down_ready:
                     down_ready.append(waits[2].wait())
@@ -472,10 +550,12 @@
     second_bufs = (*second_sums, hidden_second, *half_early)
     send_mixer = mixer_sums[0]
     feed_forward(
-        gain_first, first_gate, first_up, first_down, loads[0:3],
+        smalls[1:2], gain_first, first_gate, first_up, first_down, loads[0:3],
         first_bufs, pair_first, 0, 1,
     )
 
+    for small in smalls[2:9]:
+        small.wait()
     high, low, squares = norm_operand(gain_mixer)
     all_heads = beta_weight.shape[0]
     across = (((1,), (1,)), ((), ()))
@@ -512,15 +592,20 @@
     slot = lax.broadcasted_iota(jnp.int32, (half, LANES), 0)
     live = jnp.where(slot < lengths[0], 1.0, 0.0)
     scale, logits = None, None
+    direct = last_of(count, MIXER_DIRECT)
     branch = jnp.zeros((rows, width), F32)
     for stage, c in in_order(count):
         if stage == 0:
             rs_second(mixer_bufs, 6, c, *mixed_at(c))
             continue
         if stage == 2:
-            ag_plane(mixer_bufs, 6, c, c * size, size)
+            if c not in direct:
+                ag_near(mixer_bufs, 6, c, c * size, size)
+                ag_plane(mixer_bufs, 6, c, c * size, size)
             continue
         if stage == 3:
+            if c in direct:
+                ag_near(mixer_bufs, 6, c, c * size, size)
             ag_wait(mixer_bufs, 6, c, c * size, size)
             if c == 0:
                 loads[8].wait()
@@ -575,7 +660,7 @@
             last = reach[NEW - 1 : NEW]
             gained = update * jnp.exp(last - reach)
             zero = jnp.zeros_like(keyvec)
-            new_state[h] = old * jnp.exp(last) + lax.dot_general(
+            new_state[0, h] = old * jnp.exp(last) + lax.dot_general(
                 jnp.concatenate([keyvec, zero], axis=0),
                 jnp.concatenate([gained, zero], axis=0),
                 (((0,), (0,)), ((), ())),
@@ -589,8 +674,8 @@
                 BF16
             )
         ag_depth(mixer_bufs, 6, c, c * size, size)
-    save = pltpu.make_async_copy(new_state, state_out_hbm.at[0], load_sem.at[12])
-    save.start()
+        if c in direct:
+            ag_direct(mixer_bufs, 6, c, c * size, size)
     pair_mixer[my_tp] = branch
     all_tp(pair_mixer.at[my_tp], pair_mixer.at[my_tp], 2, pair_mixer.at[0])
     branch = pair_mixer[0]
@@ -599,14 +684,13 @@
     resid[...] = (resid[...] + branch).astype(BF16).astype(F32)
 
     feed_forward(
-        gain_second, second_gate, second_up, second_down, loads[9:12],
+        smalls[9:10], gain_second, second_gate, second_up, second_down, loads[9:12],
         second_bufs, pair_second, 12, 3,
     )
     arrived[...] = lax.dot_general(
         natural[...], resid[...].astype(BF16), (((0,), (0,)), ((), ())), preferred_element_type=F32
     )
     layer_out[...] = arrived[own, :].astype(BF16)
-    save.wait()
     all_sent(first_bufs, 0)
     all_sent(mixer_bufs, 6)
     all_sent(second_bufs, 12)
@@ -648,8 +732,7 @@
         half_parts = pieces(units // LANES, 4)
         mixer_parts = pieces(memory_state.shape[1], 4)
         vmem = pl.BlockSpec(memory_space=pltpu.VMEM)
-        smem = pl.BlockSpec(memory_space=pltpu.SMEM)
-        hbm = pl.BlockSpec(memory_space=pl.ANY)
+        hbm = pl.BlockSpec(memory_space=pltpu.HBM)
 
         def like(array):
             return pltpu.VMEM(array.shape, array.dtype)
@@ -674,19 +757,26 @@
         def pairs():
             return pltpu.VMEM((tps, rows, width), F32)
 
-        return pl.pallas_call(
+        parts = pl.pallas_call(
             functools.partial(layer_kernel, n, tps),
             name="layer",
             out_shape=(
-                jax.ShapeDtypeStruct(tokens.shape, BF16),
-                jax.ShapeDtypeStruct(memory_state.shape, F32),
+                pltpu.VMEM(tokens.shape, BF16),
+                pltpu.VMEM(memory_state.shape, F32),
             ),
-            in_specs=[
-                vmem, smem, hbm, vmem, hbm, hbm, hbm, vmem, hbm, hbm, hbm, hbm,
-                vmem, vmem, smem, smem, vmem, hbm, vmem, hbm, hbm, hbm,
-            ],
-            out_specs=(vmem, hbm),
+            in_specs=[hbm] * 22,
+            out_specs=(vmem, vmem),
             scratch_shapes=[
+                like(tokens),
+                pltpu.SMEM(lengths.shape, lengths.dtype),
+                pltpu.VMEM((1, width), F32),
+                pltpu.VMEM((1, width), F32),
+                pltpu.VMEM(beta_weight.shape[::-1], BF16),
+                pltpu.VMEM(decay_weight.shape[::-1], BF16),
+                pltpu.SMEM((1, decay_rate.shape[0]), F32),
+                pltpu.SMEM((1, decay_bias.shape[0]), F32),
+                pltpu.VMEM((1, HEAD_DIM), F32),
+                pltpu.VMEM((1, width), F32),
                 like(first_gate),
                 like(first_up),
                 like(first_down),
@@ -698,7 +788,6 @@
                 like(second_gate),
                 like(second_up),
                 like(second_down),
-                pltpu.VMEM(memory_state.shape[1:], F32),
                 pltpu.VMEM(memory_state.shape[1:], F32),
                 pltpu.VMEM((rows, width), F32),
                 pltpu.VMEM((2 * rows, rows), BF16),
@@ -714,12 +803,13 @@
                 pairs(),
                 pairs(),
                 pairs(),
-                pltpu.SemaphoreType.DMA((13,)),
+                pltpu.SemaphoreType.DMA((12,)),
                 pltpu.SemaphoreType.DMA((18,)),
                 pltpu.SemaphoreType.DMA((18, 4)),
                 pltpu.SemaphoreType.DMA((2, 4)),
                 pltpu.SemaphoreType.DMA((3,)),
                 pltpu.SemaphoreType.REGULAR((3,)),
+                pltpu.SemaphoreType.DMA((10,)),
             ],
             compiler_params=pltpu.CompilerParams(
                 collective_id=0,
@@ -750,6 +840,18 @@
             second_up,
             second_down,
         )
+        return pl.pallas_call(
+            put_out,
+            name="put_out",
+            out_shape=(
+                jax.ShapeDtypeStruct(tokens.shape, BF16),
+                jax.ShapeDtypeStruct(memory_state.shape, F32),
+            ),
+            in_specs=[vmem, vmem],
+            out_specs=(hbm, hbm),
+            scratch_shapes=[pltpu.SemaphoreType.DMA((2,))],
+            compiler_params=pltpu.CompilerParams(vmem_limit_bytes=2 * 1024 * 1024),
+        )(*parts)
 
     in_specs = (
         P("tp", "kv"),

time: 71.7 us -> 65.7 us (0.916)
  local copies, waits for them, and re-layouts: 3.17 us -> 0 us
  Pallas kernels: 67 us -> 64.3 us
    pallas_call x1, Pallas kernels: 67 us -> 63.5 us  [on_device(): pl.pallas_call(functools.partial(layer_kernel, n, tps), name='layer', out...]
    unnamed x2 -> x0, local copies, waits for them, and re-layouts: 3.17 us -> none
    pallas_call x0 -> x1, Pallas kernels: none -> 0.82 us  [on_device(): pl.pallas_call(put_out, name='put_out', out_shape=(jax.ShapeDtypeStruct(t...]
where the time goes in v2:
time: 65.7 us; the launch traced here: 65.6 us
  Pallas kernels  64.3 us (98%)
  between operations  1.29 us (2%)
    pallas_call x1, Pallas kernels, on_device(): pl.pallas_call(functools.partial(layer_kernel, n, tps), name='layer', out...  63.5 us

profile of v2, /device:TPU:0, one launch (start us, length us, event | category | flops | bytes accessed | tf_op | source)
XLA Modules:
  0.0 65.6 jit_solution(4611921976031223889)
XLA Ops:
  1.3 63.5 %layer.1 = (bf16[32,128]{1,0:T(8,128)(2,1)S(1)}, f32[1,8,128,128]{3,2,1,0:T(8,128)S(1)}) custom-call(bf16[32,128]{1,0:T(8,128)(2,1)} %tokens_hbm.1, s32[1]{0:T(128)S(6)} %copy.24.lengths_hbm, f32[1,8,128,128]{3,2,1,0:T(8,128)} %state_hbm.1, f32[1,128]{1,0:T(1,128)} %bitcast.10, bf16[128,2560]{1,0:T(8,128)(2,1)} %first_gate_hbm.1, ...), custom_call_target="tpu_custom_call" | custom-call | tf_op jit(solution)/shard_map/layer/pallas_call | solution.py:760
  64.8 0.8 %put_out.1 = (bf16[32,128]{1,0:T(8,128)(2,1)}, f32[1,8,128,128]{3,2,1,0:T(8,128)}) custom-call(bf16[32,128]{1,0:T(8,128)(2,1)S(1)} %get-tuple-element.4.layer, f32[1,8,128,128]{3,2,1,0:T(8,128)S(1)} %get-tuple-element.5.state), custom_call_target="tpu_custom_call" | custom-call | tf_op jit(solution)/shard_map/put_out/pallas_call | solution.py:843

commit v3 on v2

--- a/solution.py
+++ b/solution.py
@@ -14,7 +14,6 @@
 EPS = 1e-06
 EARLY = 1
 HALF_DIRECT = 2
-MIXER_DIRECT = 4
 F32 = jnp.float32
 BF16 = jnp.bfloat16
 
@@ -99,6 +98,7 @@
     second_up,
     second_down,
     state,
+    split,
     resid,
     spread_top,
     spread_low,
@@ -266,12 +266,6 @@
         send, mid, _, _, swap_mid, _, _, _, _, _ = bufs
         cols = pl.ds(start, size)
         stage = sems // 6
-        if paired and not swapped and c == 0:
-
-            @pl.when(late)
-            def _():
-                pl.semaphore_wait(turn_sem.at[stage], 1)
-
         if swapped:
             count, place, sem = depth, my_depth, sems + 4
         else:
@@ -301,6 +295,29 @@
 
     def early_part(bufs, start, size):
         return bufs[1].at[pl.ds(0, group - 1), :, :, pl.ds(start, size)]
+
+    def rs_begin(bufs, sems, order, sums_at, fill):
+        stage = sems // 6
+        for at, c in enumerate(order):
+            fill(c)
+            if c:
+                rs_first(bufs, sems, c, *sums_at(c))
+            if not paired:
+                if c == 0:
+                    rs_first(bufs, sems, c, *sums_at(c))
+                continue
+            if c == 0:
+
+                @pl.when(jnp.logical_not(late))
+                def _():
+                    rs_first(bufs, sems, 0, *sums_at(0))
+
+            if at == min(1, len(order) - 1):
+
+                @pl.when(late)
+                def _():
+                    pl.semaphore_wait(turn_sem.at[stage], 1)
+                    rs_first(bufs, sems, 0, *sums_at(0))
 
     def hand_over(bufs, sems, start, size):
         part = early_part(bufs, start, size)
@@ -389,7 +406,7 @@
             ).start()
             return carry
 
-        lax.fori_loop(0, depth * (group - 1), one, 0)
+        lax.fori_loop(0, depth * (group - 1), one, 0, unroll=n <= 16)
 
     def ag_plane(bufs, sems, c, start, size):
         buffer = bufs[7]
@@ -464,7 +481,7 @@
 
     def in_issue(count):
         order = list(range(count))
-        return order[-1:] + order[:-1] if swaps(count) else order
+        return order[:1] + order[-1:] + order[1:-1] if swaps(count) else order
 
     def feed_forward(before, gain, gate, up, down, waits, bufs, pair, sems, tp_sems):
         send, hidden = bufs[0], bufs[7]
@@ -482,7 +499,7 @@
             swapped = swaps(count) and c == count - 1
             return (0, LANES + size, False) if c == 0 else (LANES + c * size, size, swapped)
 
-        for c in in_issue(count):
+        def fill(c):
             for at, wide in chunks_of(size, 512):
                 lo = c * size + at
                 put(
@@ -492,7 +509,8 @@
                     jnp.dot(high, gate[:, lo : lo + wide], preferred_element_type=F32)
                     + jnp.dot(low, up[:, lo : lo + wide], preferred_element_type=F32),
                 )
-            rs_first(bufs, sems, c, *sums_at(c))
+
+        rs_begin(bufs, sems, in_issue(count), sums_at, fill)
         hand_over(bufs, sems, *sums_at(early_of(count))[:2])
         branch = jnp.zeros((rows, width), F32)
         direct = last_of(count, HALF_DIRECT)
@@ -576,7 +594,7 @@
         swapped = swaps(count) and c == count - 1
         return (0, 2 * LANES + 2 * size, False) if c == 0 else (start, 2 * size, swapped)
 
-    for c in in_issue(count):
+    def fill(c):
         for at, (first, second) in enumerate(((query_w, value_w), (key_w, outgate_w))):
             lo = c * size
             put(
@@ -586,41 +604,30 @@
                 jnp.dot(high, first[:, lo : lo + size], preferred_element_type=F32)
                 + jnp.dot(low, second[:, lo : lo + size], preferred_element_type=F32),
             )
-        rs_first(mixer_bufs, 6, c, *mixed_at(c))
+
+    rs_begin(mixer_bufs, 6, in_issue(count), mixed_at, fill)
     hand_over(mixer_bufs, 6, *mixed_at(early_of(count))[:2])
     lane = lax.broadcasted_iota(jnp.int32, (half, LANES), 1)
     slot = lax.broadcasted_iota(jnp.int32, (half, LANES), 0)
     live = jnp.where(slot < lengths[0], 1.0, 0.0)
-    scale, logits = None, None
-    direct = last_of(count, MIXER_DIRECT)
-    branch = jnp.zeros((rows, width), F32)
-    for stage, c in in_order(count):
-        if stage == 0:
-            rs_second(mixer_bufs, 6, c, *mixed_at(c))
-            continue
-        if stage == 2:
-            if c not in direct:
-                ag_near(mixer_bufs, 6, c, c * size, size)
-                ag_plane(mixer_bufs, 6, c, c * size, size)
-            continue
-        if stage == 3:
-            if c in direct:
-                ag_near(mixer_bufs, 6, c, c * size, size)
-            ag_wait(mixer_bufs, 6, c, c * size, size)
-            if c == 0:
-                loads[8].wait()
-            branch = branch + jnp.dot(
-                stacked(hidden_mixer, c * size, size),
-                out_w[c * size : (c + 1) * size, :],
-                preferred_element_type=F32,
-            )
-            continue
-        rs_wait(mixer_bufs, 6, c, *mixed_at(c))
-        if c == 0:
+    loads[7].wait()
+    for h in range(heads):
+        old = state[h]
+        top = old.astype(BF16)
+        split[h, :, :HEAD_DIM] = top
+        split[h, :, HEAD_DIM:] = (old - top.astype(F32)).astype(BF16)
+    for stage, c in in_order(count)[:count]:
+        rs_second(mixer_bufs, 6, c, *mixed_at(c))
+    groups = [range(c, min(c + 2, count)) for c in range(0, count, 2)]
+    scale, logits, grown = None, None, []
+    for group_of in groups:
+        for c in group_of:
+            rs_wait(mixer_bufs, 6, c, *mixed_at(c))
+        if scale is None:
             scale = inverse_rms(mixer_bufs)
             logits = total(mixer_bufs, LANES, LANES)
-            loads[7].wait()
-        for h in range(c * batch, (c + 1) * batch):
+        for h in range(group_of[0] * batch, (group_of[-1] + 1) * batch):
+            c = h // batch
             base = 2 * LANES + 2 * c * size + (h - c * batch) * HEAD_DIM
             both = total(mixer_bufs, base, HEAD_DIM)
             query, value = silu(both[:half] * scale), silu(both[half:] * scale)
@@ -641,12 +648,17 @@
             for i in range(NEW):
                 reach = reach + jnp.where(slot >= i, decay[i : i + 1], 0.0)
             before = jnp.exp(reach)
-            old = state[h]
-            held = jnp.dot(
-                jnp.concatenate([keyvec, query], axis=0),
-                old,
-                precision=lax.Precision.HIGHEST,
+            asked = jnp.concatenate([keyvec, query], axis=0)
+            top = asked.astype(BF16).astype(F32)
+            found = jnp.dot(
+                jnp.concatenate([top, asked - top], axis=0).astype(BF16),
+                split[h],
                 preferred_element_type=F32,
+            )
+            held = (
+                found[: 2 * half, :HEAD_DIM]
+                + found[2 * half :, :HEAD_DIM]
+                + found[: 2 * half, HEAD_DIM:]
             )
             update = beta * (value - before * held[:half])
             output = before * held[half:]
@@ -658,24 +670,36 @@
                 update = update - jnp.where(slot > i, beta * between * alike * fixed, 0.0)
                 output = output + between * jnp.sum(query * row, axis=1, keepdims=True) * fixed
             last = reach[NEW - 1 : NEW]
-            gained = update * jnp.exp(last - reach)
-            zero = jnp.zeros_like(keyvec)
-            new_state[0, h] = old * jnp.exp(last) + lax.dot_general(
-                jnp.concatenate([keyvec, zero], axis=0),
-                jnp.concatenate([gained, zero], axis=0),
-                (((0,), (0,)), ((), ())),
-                precision=lax.Precision.HIGHEST,
-                preferred_element_type=F32,
-            )
+            grown.append((keyvec, update * jnp.exp(last - reach), jnp.exp(last)))
             output = output * live
             output = output * lax.rsqrt(jnp.mean(output * output, axis=1, keepdims=True) + EPS)
             output = output * head_gain[...] * outgate
             hidden_mixer[my_plane, my_depth, :, h * HEAD_DIM : (h + 1) * HEAD_DIM] = output.astype(
                 BF16
             )
-        ag_depth(mixer_bufs, 6, c, c * size, size)
-        if c in direct:
-            ag_direct(mixer_bufs, 6, c, c * size, size)
+        part = (group_of[0], group_of[0] * size, len(group_of) * size)
+        ag_depth(mixer_bufs, 6, *part)
+        ag_direct(mixer_bufs, 6, *part)
+    for h, (keyvec, gained, kept) in enumerate(grown):
+        zero = jnp.zeros_like(keyvec)
+        new_state[0, h] = state[h] * kept + lax.dot_general(
+            jnp.concatenate([keyvec, zero], axis=0),
+            jnp.concatenate([gained, zero], axis=0),
+            (((0,), (0,)), ((), ())),
+            precision=lax.Precision.HIGHEST,
+            preferred_element_type=F32,
+        )
+    loads[8].wait()
+    branch = jnp.zeros((rows, width), F32)
+    for group_of in groups:
+        start, wide = group_of[0] * size, len(group_of) * size
+        ag_near(mixer_bufs, 6, group_of[0], start, wide)
+        ag_wait(mixer_bufs, 6, group_of[0], start, wide)
+        branch = branch + jnp.dot(
+            stacked(hidden_mixer, start, wide),
+            out_w[start : start + wide, :],
+            preferred_element_type=F32,
+        )
     pair_mixer[my_tp] = branch
     all_tp(pair_mixer.at[my_tp], pair_mixer.at[my_tp], 2, pair_mixer.at[0])
     branch = pair_mixer[0]
@@ -789,6 +813,7 @@
                 like(second_up),
                 like(second_down),
                 pltpu.VMEM(memory_state.shape[1:], F32),
+                pltpu.VMEM((*memory_state.shape[1:3], 2 * HEAD_DIM), BF16),
                 pltpu.VMEM((rows, width), F32),
                 pltpu.VMEM((2 * rows, rows), BF16),
                 pltpu.VMEM((2 * rows, rows), BF16),

time: 65.7 us -> 63.6 us (0.968)
  Pallas kernels: 64.3 us -> 62.2 us
    pallas_call x1, Pallas kernels: 63.5 us -> 61.4 us  [on_device(): pl.pallas_call(functools.partial(layer_kernel, n, tps), name='layer', out...]
where the time goes in v3:
time: 63.6 us; the launch traced here: 63.5 us
  Pallas kernels  62.2 us (98%)
  between operations  1.29 us (2%)
    pallas_call x1, Pallas kernels, on_device(): pl.pallas_call(functools.partial(layer_kernel, n, tps), name='layer', out...  61.4 us

profile of v3, /device:TPU:0, one launch (start us, length us, event | category | flops | bytes accessed | tf_op | source)
XLA Modules:
  0.0 63.5 jit_solution(8496432750529817539)
XLA Ops:
  1.3 61.4 %layer.1 = (bf16[32,128]{1,0:T(8,128)(2,1)S(1)}, f32[1,8,128,128]{3,2,1,0:T(8,128)S(1)}) custom-call(bf16[32,128]{1,0:T(8,128)(2,1)} %tokens_hbm.1, s32[1]{0:T(128)S(6)} %copy.24.lengths_hbm, f32[1,8,128,128]{3,2,1,0:T(8,128)} %state_hbm.1, f32[1,128]{1,0:T(1,128)} %bitcast.10, bf16[128,2560]{1,0:T(8,128)(2,1)} %first_gate_hbm.1, ...), custom_call_target="tpu_custom_call" | custom-call | tf_op jit(solution)/shard_map/layer/pallas_call | solution.py:784
  62.7 0.8 %put_out.1 = (bf16[32,128]{1,0:T(8,128)(2,1)}, f32[1,8,128,128]{3,2,1,0:T(8,128)}) custom-call(bf16[32,128]{1,0:T(8,128)(2,1)S(1)} %get-tuple-element.4.layer, f32[1,8,128,128]{3,2,1,0:T(8,128)S(1)} %get-tuple-element.5.state), custom_call_target="tpu_custom_call" | custom-call | tf_op jit(solution)/shard_map/put_out/pallas_call | solution.py:868

commit v4 on v3

--- a/solution.py
+++ b/solution.py
@@ -12,8 +12,10 @@
 LANES = 128
 NEW = 4
 EPS = 1e-06
+SHIFT = ((0, -1), (1, -1), (2, 2))
+HEAD_CUT = 2
 EARLY = 1
-HALF_DIRECT = 2
+HALF_DIRECT = (2, 1)
 F32 = jnp.float32
 BF16 = jnp.bfloat16
 
@@ -28,6 +30,17 @@
 
 def swaps(count):
     return count > 2
+
+
+def shares(units, count):
+    tiles = units // LANES // count
+    if swaps(count) and tiles > 3:
+        parts = [tiles] * count
+        for c, more in SHIFT:
+            parts[c] += more
+    else:
+        parts = [tiles] * count
+    return [part * LANES for part in parts]
 
 
 def early_of(count):
@@ -152,8 +165,8 @@
         )
         return carry
 
-    lax.fori_loop(1, depth, greet_depth, 0)
-    lax.fori_loop(1, group, greet_plane, 0)
+    lax.fori_loop(1, depth, greet_depth, 0, unroll=depth <= 4)
+    lax.fori_loop(1, group, greet_plane, 0, unroll=group <= 4)
     lax.fori_loop(1, tps, greet_tp, 0)
 
     smalls = []
@@ -291,33 +304,44 @@
             ).start()
             return carry
 
-        lax.fori_loop(1, count, one, 0)
+        lax.fori_loop(1, count, one, 0, unroll=count <= 4)
 
     def early_part(bufs, start, size):
         return bufs[1].at[pl.ds(0, group - 1), :, :, pl.ds(start, size)]
 
-    def rs_begin(bufs, sems, order, sums_at, fill):
-        stage = sems // 6
+    def rs_begin(bufs, sems, order, sums_at, fill, sizes, header, cut):
+        def head(begin, end):
+            rs_first(bufs, sems, 0, begin, end - begin, False)
+
+        whole = header + sizes[0]
+        first = header + cut
         for at, c in enumerate(order):
-            fill(c)
             if c:
+                fill(c, 0, sizes[c])
                 rs_first(bufs, sems, c, *sums_at(c))
-            if not paired:
-                if c == 0:
-                    rs_first(bufs, sems, c, *sums_at(c))
-                continue
-            if c == 0:
+            elif not paired:
+                fill(0, 0, sizes[0])
+                head(0, whole)
+            else:
+                fill(0, 0, cut)
 
                 @pl.when(jnp.logical_not(late))
                 def _():
-                    rs_first(bufs, sems, 0, *sums_at(0))
-
-            if at == min(1, len(order) - 1):
+                    head(0, first)
+
+                if first < whole:
+                    fill(0, cut, sizes[0])
+
+                    @pl.when(jnp.logical_not(late))
+                    def _():
+                        head(first, whole)
+
+            if paired and at == min(1, len(order) - 1):
 
                 @pl.when(late)
                 def _():
-                    pl.semaphore_wait(turn_sem.at[stage], 1)
-                    rs_first(bufs, sems, 0, *sums_at(0))
+                    pl.semaphore_wait(turn_sem.at[sems // 6], 1)
+                    head(0, whole)
 
     def hand_over(bufs, sems, start, size):
         part = early_part(bufs, start, size)
@@ -365,7 +389,7 @@
             ).start()
             return carry
 
-        lax.fori_loop(1, count, one, 0)
+        lax.fori_loop(1, count, one, 0, unroll=count <= 4)
 
     def rs_wait(bufs, sems, c, start, size, swapped):
         part = bufs[6] if swapped else bufs[3].at[:, :, pl.ds(start, size)]
@@ -386,7 +410,7 @@
             ).start()
             return carry
 
-        lax.fori_loop(1, depth, one, 0)
+        lax.fori_loop(1, depth, one, 0, unroll=depth <= 4)
 
     def ag_direct(bufs, sems, c, start, size):
         buffer = bufs[7]
@@ -424,7 +448,7 @@
             ).start()
             return carry
 
-        lax.fori_loop(1, group, one, 0)
+        lax.fori_loop(1, group, one, 0, unroll=group <= 4)
 
     def ag_near(bufs, sems, c, start, size):
         part = bufs[7].at[0, pl.ds(0, depth - 1), :, pl.ds(start, size)]
@@ -490,18 +514,21 @@
         high, low, squares = norm_operand(gain)
         units = gate.shape[1]
         count = pieces(units // LANES, 4)
-        size = units // count
+        sizes = shares(units, count)
+        starts = [sum(sizes[:c]) for c in range(count)]
         put(send, 0, LANES, squares)
         waits[0].wait()
         waits[1].wait()
 
         def sums_at(c):
             swapped = swaps(count) and c == count - 1
-            return (0, LANES + size, False) if c == 0 else (LANES + c * size, size, swapped)
-
-        def fill(c):
-            for at, wide in chunks_of(size, 512):
-                lo = c * size + at
+            if c == 0:
+                return 0, LANES + sizes[0], False
+            return LANES + starts[c], sizes[c], swapped
+
+        def fill(c, begin, end):
+            for at, wide in chunks_of(end - begin, 512):
+                lo = starts[c] + begin + at
                 put(
                     send,
                     LANES + lo,
@@ -510,10 +537,23 @@
                     + jnp.dot(low, up[:, lo : lo + wide], preferred_element_type=F32),
                 )
 
-        rs_begin(bufs, sems, in_issue(count), sums_at, fill)
+        cut = min(HEAD_CUT * LANES, sizes[0])
+        rs_begin(bufs, sems, in_issue(count), sums_at, fill, sizes, LANES, cut)
         hand_over(bufs, sems, *sums_at(early_of(count))[:2])
         branch = jnp.zeros((rows, width), F32)
-        direct = last_of(count, HALF_DIRECT)
+        slow = last_of(count, HALF_DIRECT[0])
+        fast = last_of(count, HALF_DIRECT[1]) if paired else slow
+
+        def where(c, wanted, step, *span):
+            on_slow, on_fast = (c in slow) == wanted, (c in fast) == wanted
+            if on_slow and on_fast:
+                step(bufs, sems, c, *span)
+            elif on_slow or on_fast:
+
+                @pl.when(late if on_fast else jnp.logical_not(late))
+                def _():
+                    step(bufs, sems, c, *span)
+
         scale, down_ready = None, []
         for stage, c in in_order(count):
             if stage == 0:
@@ -522,28 +562,25 @@
                 rs_wait(bufs, sems, c, *sums_at(c))
                 if c == 0:
                     scale = inverse_rms(bufs)
-                for at, wide in chunks_of(size, LANES):
-                    lo = c * size + at
+                for at, wide in chunks_of(sizes[c], LANES):
+                    lo = starts[c] + at
                     both = total(bufs, LANES + lo, wide)
                     hidden[my_plane, my_depth, :, lo : lo + wide] = (
                         silu(both[:half] * scale) * (both[half:] * scale)
                     ).astype(BF16)
-                ag_depth(bufs, sems, c, c * size, size)
-                if c in direct:
-                    ag_direct(bufs, sems, c, c * size, size)
+                ag_depth(bufs, sems, c, starts[c], sizes[c])
+                where(c, True, ag_direct, starts[c], sizes[c])
             elif stage == 2:
-                if c not in direct:
-                    ag_near(bufs, sems, c, c * size, size)
-                    ag_plane(bufs, sems, c, c * size, size)
+                where(c, False, ag_near, starts[c], sizes[c])
+                where(c, False, ag_plane, starts[c], sizes[c])
             else:
-                if c in direct:
-                    ag_near(bufs, sems, c, c * size, size)
-                ag_wait(bufs, sems, c, c * size, size)
+                where(c, True, ag_near, starts[c], sizes[c])
+                ag_wait(bufs, sems, c, starts[c], sizes[c])
                 if not down_ready:
                     down_ready.append(waits[2].wait())
                 branch = branch + jnp.dot(
-                    stacked(hidden, c * size, size),
-                    down[c * size : (c + 1) * size, :],
+                    stacked(hidden, starts[c], sizes[c]),
+                    down[starts[c] : starts[c] + sizes[c], :],
                     preferred_element_type=F32,
                 )
         pair[my_tp] = branch
@@ -554,15 +591,16 @@
         resid[...] = (resid[...] + 0.5 * branch).astype(BF16).astype(F32)
 
     half_count = pieces(first_gate.shape[1] // LANES, 4)
-    half_size = first_gate.shape[1] // half_count
+    half_sizes = shares(first_gate.shape[1], half_count)
     mixer_count = pieces(heads, 4)
     mixer_size = 2 * heads * HEAD_DIM // mixer_count
 
-    def early_width(before, parts, each):
-        return each if early_of(parts) else before + each
-
-    half_early = (half_count, early_width(LANES, half_count, half_size))
-    mixer_early = (mixer_count, early_width(2 * LANES, mixer_count, mixer_size))
+    def early_width(before, sizes):
+        at = early_of(len(sizes))
+        return sizes[at] if at else before + sizes[0]
+
+    half_early = (half_count, early_width(LANES, half_sizes))
+    mixer_early = (mixer_count, early_width(2 * LANES, [mixer_size] * mixer_count))
     first_bufs = (*first_sums, hidden_first, *half_early)
     mixer_bufs = (*mixer_sums, hidden_mixer, *mixer_early)
     second_bufs = (*second_sums, hidden_second, *half_early)
@@ -594,8 +632,10 @@
         swapped = swaps(count) and c == count - 1
         return (0, 2 * LANES + 2 * size, False) if c == 0 else (start, 2 * size, swapped)
 
-    def fill(c):
+    def fill(c, begin, end):
         for at, (first, second) in enumerate(((query_w, value_w), (key_w, outgate_w))):
+            if not begin <= at * size < end:
+                continue
             lo = c * size
             put(
                 send_mixer,
@@ -605,7 +645,9 @@
                 + jnp.dot(low, second[:, lo : lo + size], preferred_element_type=F32),
             )
 
-    rs_begin(mixer_bufs, 6, in_issue(count), mixed_at, fill)
+    rs_begin(
+        mixer_bufs, 6, in_issue(count), mixed_at, fill, [2 * size] * count, 2 * LANES, size
+    )
     hand_over(mixer_bufs, 6, *mixed_at(early_of(count))[:2])
     lane = lax.broadcasted_iota(jnp.int32, (half, LANES), 1)
     slot = lax.broadcasted_iota(jnp.int32, (half, LANES), 0)
@@ -761,10 +803,11 @@
         def like(array):
             return pltpu.VMEM(array.shape, array.dtype)
 
-        def owners(before, parts, each):
-            last = each if swaps(parts) else LANES
-            columns = before + parts * each
-            kept = columns - (last if swaps(parts) else 0)
+        def owners(before, sizes):
+            swapped = swaps(len(sizes))
+            last = sizes[-1] if swapped else LANES
+            columns = before + sum(sizes)
+            kept = columns - (last if swapped else 0)
             return (
                 pltpu.VMEM((group, depth, 2 * NEW, columns), BF16),
                 pltpu.VMEM((group, depth, 2 * NEW, kept), BF16),
@@ -819,9 +862,9 @@
                 pltpu.VMEM((2 * rows, rows), BF16),
                 pltpu.VMEM((rows, width), F32),
                 pltpu.VMEM((rows, rows), BF16),
-                owners(LANES, half_parts, units // half_parts),
-                owners(2 * LANES, mixer_parts, 2 * span // mixer_parts),
-                owners(LANES, half_parts, units // half_parts),
+                owners(LANES, shares(units, half_parts)),
+                owners(2 * LANES, [2 * span // mixer_parts] * mixer_parts),
+                owners(LANES, shares(units, half_parts)),
                 gathered(units),
                 gathered(span),
                 gathered(units),

time: 63.6 us -> 63 us (level)
  Pallas kernels: 62.2 us -> 61.5 us
    pallas_call x1, Pallas kernels: 61.4 us -> 60.7 us  [on_device(): pl.pallas_call(functools.partial(layer_kernel, n, tps), name='layer', out...]
where the time goes in v4:
time: 63 us; the launch traced here: 62.8 us
  Pallas kernels  61.5 us (98%)
  between operations  1.29 us (2%)
    pallas_call x1, Pallas kernels, on_device(): pl.pallas_call(functools.partial(layer_kernel, n, tps), name='layer', out...  60.7 us

profile of v4, /device:TPU:0, one launch (start us, length us, event | category | flops | bytes accessed | tf_op | source)
XLA Modules:
  0.0 62.8 jit_solution(4940987339070975225)
XLA Ops:
  1.3 60.7 %layer.1 = (bf16[32,128]{1,0:T(8,128)(2,1)S(1)}, f32[1,8,128,128]{3,2,1,0:T(8,128)S(1)}) custom-call(bf16[32,128]{1,0:T(8,128)(2,1)} %tokens_hbm.1, s32[1]{0:T(128)S(6)} %copy.24.lengths_hbm, f32[1,8,128,128]{3,2,1,0:T(8,128)} %state_hbm.1, f32[1,128]{1,0:T(1,128)} %bitcast.10, bf16[128,2560]{1,0:T(8,128)(2,1)} %first_gate_hbm.1, ...), custom_call_target="tpu_custom_call" | custom-call | tf_op jit(solution)/shard_map/layer/pallas_call | solution.py:827
  62.0 0.8 %put_out.1 = (bf16[32,128]{1,0:T(8,128)(2,1)}, f32[1,8,128,128]{3,2,1,0:T(8,128)}) custom-call(bf16[32,128]{1,0:T(8,128)(2,1)S(1)} %get-tuple-element.4.layer, f32[1,8,128,128]{3,2,1,0:T(8,128)S(1)} %get-tuple-element.5.state), custom_call_target="tpu_custom_call" | custom-call | tf_op jit(solution)/shard_map/put_out/pallas_call | solution.py:911

commit v5 on v4

--- a/solution.py
+++ b/solution.py
@@ -218,6 +218,7 @@
     spread_top[...] = jnp.where(hit & top, 1.0, 0.0).astype(BF16)
     spread_low[...] = jnp.where(hit & jnp.logical_not(top), 1.0, 0.0).astype(BF16)
 
+    mixer_sums[0][:, :, :, LANES : 2 * LANES] = jnp.zeros((group, depth, 2 * half, LANES), BF16)
     smalls[0].wait()
     own = pl.ds(pl.multiple_of(my_tp * own_rows, own_rows), own_rows)
     arrived[own, :] = tokens[...].astype(F32)
@@ -309,7 +310,7 @@
     def early_part(bufs, start, size):
         return bufs[1].at[pl.ds(0, group - 1), :, :, pl.ds(start, size)]
 
-    def rs_begin(bufs, sems, order, sums_at, fill, sizes, header, cut):
+    def rs_begin(bufs, sems, order, sums_at, fill, sizes, header, cut, put_header=None):
         def head(begin, end):
             rs_first(bufs, sems, 0, begin, end - begin, False)
 
@@ -320,6 +321,8 @@
                 fill(c, 0, sizes[c])
                 rs_first(bufs, sems, c, *sums_at(c))
             elif not paired:
+                if put_header:
+                    put_header()
                 fill(0, 0, sizes[0])
                 head(0, whole)
             else:
@@ -327,7 +330,14 @@
 
                 @pl.when(jnp.logical_not(late))
                 def _():
-                    head(0, first)
+                    head(header if put_header else 0, first)
+
+                if put_header:
+                    put_header()
+
+                    @pl.when(jnp.logical_not(late))
+                    def _():
+                        head(0, header)
 
                 if first < whole:
                     fill(0, cut, sizes[0])
@@ -615,12 +625,14 @@
     high, low, squares = norm_operand(gain_mixer)
     all_heads = beta_weight.shape[0]
     across = (((1,), (1,)), ((), ()))
-    put(send_mixer, 0, LANES, squares)
-    send_mixer[:, :, :, LANES : 2 * LANES] = jnp.zeros((group, depth, 2 * half, LANES), BF16)
-    small = lax.dot_general(
-        high, beta_weight[...], across, preferred_element_type=F32
-    ) + lax.dot_general(low, decay_weight[...], across, preferred_element_type=F32)
-    put(send_mixer, LANES, all_heads, small)
+
+    def put_header():
+        small = lax.dot_general(
+            high, beta_weight[...], across, preferred_element_type=F32
+        ) + lax.dot_general(low, decay_weight[...], across, preferred_element_type=F32)
+        put(send_mixer, 0, LANES, squares)
+        put(send_mixer, LANES, all_heads, small)
+
     for load in loads[3:7]:
         load.wait()
     count = pieces(heads, 4)
@@ -646,7 +658,8 @@
             )
 
     rs_begin(
-        mixer_bufs, 6, in_issue(count), mixed_at, fill, [2 * size] * count, 2 * LANES, size
+        mixer_bufs, 6, in_issue(count), mixed_at, fill, [2 * size] * count, 2 * LANES, size,
+        put_header,
     )
     hand_over(mixer_bufs, 6, *mixed_at(early_of(count))[:2])
     lane = lax.broadcasted_iota(jnp.int32, (half, LANES), 1)

time: 63 us -> 63.2 us (level)
  no operation moved by 1% of the time
where the time goes in v5:
time: 63.2 us; the launch traced here: 63 us
  Pallas kernels  61.7 us (98%)
  between operations  1.29 us (2%)
    pallas_call x1, Pallas kernels, on_device(): pl.pallas_call(functools.partial(layer_kernel, n, tps), name='layer', out...  60.9 us

profile of v5, /device:TPU:0, one launch (start us, length us, event | category | flops | bytes accessed | tf_op | source)
XLA Modules:
  0.0 63.0 jit_solution(12033795541865672365)
XLA Ops:
  1.3 60.9 %layer.1 = (bf16[32,128]{1,0:T(8,128)(2,1)S(1)}, f32[1,8,128,128]{3,2,1,0:T(8,128)S(1)}) custom-call(bf16[32,128]{1,0:T(8,128)(2,1)} %tokens_hbm.1, s32[1]{0:T(128)S(6)} %copy.24.lengths_hbm, f32[1,8,128,128]{3,2,1,0:T(8,128)} %state_hbm.1, f32[1,128]{1,0:T(1,128)} %bitcast.10, bf16[128,2560]{1,0:T(8,128)(2,1)} %first_gate_hbm.1, ...), custom_call_target="tpu_custom_call" | custom-call | tf_op jit(solution)/shard_map/layer/pallas_call | solution.py:840
  62.2 0.8 %put_out.1 = (bf16[32,128]{1,0:T(8,128)(2,1)}, f32[1,8,128,128]{3,2,1,0:T(8,128)}) custom-call(bf16[32,128]{1,0:T(8,128)(2,1)S(1)} %get-tuple-element.4.layer, f32[1,8,128,128]{3,2,1,0:T(8,128)S(1)} %get-tuple-element.5.state), custom_call_target="tpu_custom_call" | custom-call | tf_op jit(solution)/shard_map/put_out/pallas_call | solution.py:924
